TPU v7x, 32 devices: a whole 2x2x4 slice. The times are simulated.
32 devices in a mesh: sp: 16 (over z, y, x), tp: 2 (over core).
Axes of the slice: x: 2, y: 2, z: 4, core: 2. Of those that a mesh axis runs over, the one named last changes fastest.
Arguments:
- queries: bfloat16 [1, 6144, 2048], P(None, 'sp', 'tp'), may hold values from -5 to 5
- keys: bfloat16 [1, 6144, 2048], P(None, 'sp', 'tp'), may hold values from -5 to 5
- values: bfloat16 [1, 6144, 2048], P(None, 'sp', 'tp'), may hold values from -6 to 6
- rel_bias: float32 [16, 192], P('tp'), may hold values from -3 to 3
- out_grad: bfloat16 [1, 6144, 2048], P(None, 'sp', 'tp'), may hold values from -48 to 48
Outputs:
- query_grad: bfloat16 [1, 6144, 2048], P(None, 'sp', 'tp')
- key_grad: bfloat16 [1, 6144, 2048], P(None, 'sp', 'tp')
- value_grad: bfloat16 [1, 6144, 2048], P(None, 'sp', 'tp')
- bias_grad: float32 [16, 192], replicated
All inputs are finite; a program needn't handle non-finite values.
Results may differ from a plain program's by a relative error of at most 0.0049.
Values may be sent and summed in bfloat16 or wider, within the bound.
A program may use at most 64 MiB of HBM per device.

v0:
```python
import jax
import jax.numpy as jnp
from jax import lax
from jax.sharding import PartitionSpec as P

HEAD_DIM = 128
SEG = 64
LEFT = 4
CLIP = 128
BAND = 320
BUCKETS = 192


def from_behind(value, axis, steps):
    count = lax.axis_size(axis)
    leading, last = (max(0, -steps), min(count, count - steps))
    return lax.ppermute(value, axis, [(source, source + steps) for source in range(leading, last)])


def diagonal_onehot():
    span = SEG + BAND - 1
    diag = jnp.arange(span, dtype=jnp.int32)
    bucket = jnp.clip(SEG - 1 - diag + LEFT * SEG, 1 - SEG, CLIP) + SEG - 1
    return (bucket[None, :] == jnp.arange(BUCKETS, dtype=jnp.int32)[:, None]).astype(jnp.float32)


def on_diagonals(rel_bias, onehot):
    return jnp.dot(
        rel_bias, onehot, preferred_element_type=jnp.float32, precision=lax.Precision.HIGHEST
    )


def fill_toeplitz(diag_vals):
    head_count, span = diag_vals.shape
    tiled = jnp.tile(diag_vals, (1, SEG))[:, SEG - 1 :]
    tiled = tiled[:, : SEG * (span - 1)].reshape(head_count, SEG, span - 1)
    return tiled[:, :, :BAND]


def sum_diagonals(terms):
    head_count = terms.shape[0]
    span = SEG + BAND - 1
    padded = jnp.concatenate(
        [
            jnp.zeros((head_count, SEG, SEG - 1), jnp.float32),
            terms,
            jnp.zeros((head_count, SEG, SEG), jnp.float32),
        ],
        axis=2,
    )
    width = padded.shape[2]
    flat = jnp.concatenate(
        [padded.reshape(head_count, SEG * width), jnp.zeros((head_count, SEG), jnp.float32)], axis=1
    )
    skewed = flat.reshape(head_count, SEG, width + 1)[:, :, :span]
    return jnp.sum(skewed, axis=1)


def band_core(q_segs, k_band, v_band, g_segs, table, key_valid):
    seg_count = q_segs.shape[1]
    score_scale = HEAD_DIM ** (-0.5)
    score_parts = []
    prob_parts = []
    for offset in range(LEFT + 1):
        score_parts.append(
            jnp.einsum(
                "sncha,snkha->snhck",
                q_segs,
                k_band[:, offset : offset + seg_count],
                preferred_element_type=jnp.float32,
            )
        )
        prob_parts.append(
            jnp.einsum(
                "sncha,snkha->snhck",
                g_segs,
                v_band[:, offset : offset + seg_count],
                preferred_element_type=jnp.float32,
            )
        )
    score = jnp.concatenate(score_parts, axis=-1) * score_scale + table[None, None]
    score = jnp.where(key_valid[None, :, None, None, :], score, -jnp.inf)
    row_max = jnp.max(score, axis=-1, keepdims=True)
    expo = jnp.exp(score - row_max)
    row_sum = jnp.sum(expo, axis=-1, keepdims=True)
    prob = expo / row_sum
    log_norm = (row_max + jnp.log(row_sum))[..., 0]
    prob_grad = jnp.concatenate(prob_parts, axis=-1)
    row_delta = jnp.sum(prob * prob_grad, axis=-1)
    score_grad = prob * (prob_grad - row_delta[..., None])
    bias_terms = jnp.sum(score_grad, axis=(0, 1))
    prob_low = prob.astype(jnp.bfloat16)
    grad_low = (score_grad * score_scale).astype(jnp.bfloat16)
    query_acc = jnp.zeros(q_segs.shape, jnp.float32)
    key_acc = jnp.zeros(k_band.shape, jnp.float32)
    value_acc = jnp.zeros(k_band.shape, jnp.float32)
    for offset in range(LEFT + 1):
        grad_part = grad_low[..., offset * SEG : (offset + 1) * SEG]
        prob_part = prob_low[..., offset * SEG : (offset + 1) * SEG]
        query_acc = query_acc + jnp.einsum(
            "snhck,snkha->sncha",
            grad_part,
            k_band[:, offset : offset + seg_count],
            preferred_element_type=jnp.float32,
        )
        first_seg = 0
        key_acc = key_acc.at[:, offset + first_seg : offset + seg_count].add(
            jnp.einsum("snhck,sncha->snkha", grad_part, q_segs, preferred_element_type=jnp.float32)
        )
        value_acc = value_acc.at[:, offset + first_seg : offset + seg_count].add(
            jnp.einsum("snhck,sncha->snkha", prob_part, g_segs, preferred_element_type=jnp.float32)
        )
    return (query_acc, key_acc, value_acc, bias_terms, log_norm, row_delta)


def local(queries, keys, values, rel_bias, out_grad):
    seq_count, tok_rows, row_width = queries.shape
    head_count = row_width // HEAD_DIM
    seg_count = tok_rows // SEG
    reach = LEFT * SEG
    seq_index = lax.axis_index("sp")
    seg_shape = (seq_count, seg_count, SEG, head_count, HEAD_DIM)
    band_shape = (seq_count, seg_count + LEFT, SEG, head_count, HEAD_DIM)
    onehot = diagonal_onehot()
    table = fill_toeplitz(on_diagonals(rel_bias, onehot))
    prior_k, prior_v = from_behind(
        (keys[:, tok_rows - reach :], values[:, tok_rows - reach :]), "sp", 1
    )
    k_band = jnp.concatenate([prior_k, keys], axis=1).reshape(band_shape)
    v_band = jnp.concatenate([prior_v, values], axis=1).reshape(band_shape)
    q_segs = queries.reshape(seg_shape)
    g_segs = out_grad.reshape(seg_shape)
    positions = (
        seq_index * tok_rows
        + jnp.arange(seg_count, dtype=jnp.int32)[:, None] * SEG
        - reach
        + jnp.arange(BAND, dtype=jnp.int32)[None, :]
    )
    key_valid = positions >= 0
    flat = (seq_count, reach + tok_rows, row_width)
    query_acc, key_acc, value_acc, bias_terms, log_norm, row_delta = band_core(
        q_segs, k_band, v_band, g_segs, table, key_valid
    )
    key_flat = key_acc.reshape(flat)
    value_flat = value_acc.reshape(flat)
    back_k, back_v = from_behind((key_flat[:, :reach], value_flat[:, :reach]), "sp", -1)
    key_own = key_flat[:, reach:].at[:, tok_rows - reach :].add(back_k)
    value_own = value_flat[:, reach:].at[:, tok_rows - reach :].add(back_v)
    query_grad = query_acc.astype(jnp.bfloat16).reshape(seq_count, tok_rows, row_width)
    key_grad = key_own.astype(jnp.bfloat16)
    value_grad = value_own.astype(jnp.bfloat16)
    local_bias = jnp.dot(
        sum_diagonals(bias_terms),
        onehot.T,
        preferred_element_type=jnp.float32,
        precision=lax.Precision.HIGHEST,
    )
    full_table = jnp.zeros((head_count * lax.axis_size("tp"), BUCKETS), jnp.float32)
    full_table = lax.dynamic_update_slice_in_dim(
        full_table, local_bias, lax.axis_index("tp") * head_count, 0
    )
    bias_grad = lax.psum(full_table, ("sp", "tp"))
    return (query_grad, key_grad, value_grad, bias_grad)


def solution(mesh):
    return jax.shard_map(
        local,
        mesh=mesh,
        in_specs=(
            P(None, "sp", "tp"),
            P(None, "sp", "tp"),
            P(None, "sp", "tp"),
            P("tp", None),
            P(None, "sp", "tp"),
        ),
        out_specs=(P(None, "sp", "tp"), P(None, "sp", "tp"), P(None, "sp", "tp"), P()),
        check_vma=False,
    )
```

profile of v0, /device:TPU:0, one launch (start us, length us, event | category | flops | bytes accessed | tf_op | source)
XLA Modules:
  0.0 184.4 jit_solution(14857570000628562760)
XLA Ops:
  0.7 2.0 %slice.478 = bf16[1,256,1024]{2,1,0:T(8,128)(2,1)} slice(bf16[1,384,1024]{2,1,0:T(8,128)(2,1)} %param.30), slice={[0:1], [128:384], [0:1024]} | slice | bytes 1048576 | tf_op jit(solution)/shard_map/slice | solution.py:127
  2.7 5.7 %collective-permute-start = (bf16[1,256,1024]{2,1,0:T(8,128)(2,1)}, bf16[1,256,1024]{2,1,0:T(8,128)(2,1)}, u32[]{:S(2)}, u32[]{:S(2)}) collective-permute-start(bf16[1,256,1024]{2,1,0:T(8,128)(2,1)} %slice.478), channel_id=1, source_target_pairs={{0,2},{2,4},{4,6},{6,8},{8,10},{10,12},{12,14},{14,16},{16,18},{18... | collective-permute-start | bytes 1572872 | tf_op jit(solution)/shard_map/ppermute | solution.py:17
  8.3 1.9 %slice.486 = bf16[1,256,1024]{2,1,0:T(8,128)(2,1)} slice(bf16[1,384,1024]{2,1,0:T(8,128)(2,1)} %param.31), slice={[0:1], [128:384], [0:1024]} | slice | bytes 1048576 | tf_op jit(solution)/shard_map/slice | solution.py:127
  10.2 3.4 %collective-permute-start.1 = (bf16[1,256,1024]{2,1,0:T(8,128)(2,1)}, bf16[1,256,1024]{2,1,0:T(8,128)(2,1)}, u32[]{:S(2)}, u32[]{:S(2)}) collective-permute-start(bf16[1,256,1024]{2,1,0:T(8,128)(2,1)} %slice.486), channel_id=1, source_target_pairs={{0,2},{2,4},{4,6},{6,8},{8,10},{10,12},{12,14},{14,16},{16,18},{18... | collective-permute-start | bytes 1572872 | tf_op jit(solution)/shard_map/ppermute | solution.py:17
  16.0 2.0 %reshape.1124 = f32[8,64,382]{2,1,0:T(8,128)S(1)} reshape(f32[8,24448]{1,0:T(8,128)} %slice.522) | data formatting | bytes 1564672 | tf_op jit(solution)/shard_map/reshape | solution.py:36
  18.1 2.1 %collective-permute-done = bf16[1,256,1024]{2,1,0:T(8,128)(2,1)} collective-permute-done((bf16[1,256,1024]{2,1,0:T(8,128)(2,1)}, bf16[1,256,1024]{2,1,0:T(8,128)(2,1)}, u32[]{:S(2)}, u32[]{:S(2)}) %collective-permute-start) | collective-permute-done | bytes 524320 | tf_op jit(solution)/shard_map/ppermute | solution.py:17
  22.8 7.4 %collective-permute-done.1 = bf16[1,256,1024]{2,1,0:T(8,128)(2,1)} collective-permute-done((bf16[1,256,1024]{2,1,0:T(8,128)(2,1)}, bf16[1,256,1024]{2,1,0:T(8,128)(2,1)}, u32[]{:S(2)}, u32[]{:S(2)}) %collective-permute-start.1) | collective-permute-done | bytes 524320 | tf_op jit(solution)/shard_map/ppermute | solution.py:17
  44.5 1.8 convolution_bitcast_fusion.9
  49.7 6.9 %concatenate.116 = f32[1,6,8,64,320]{4,3,2,1,0:T(8,128)} concatenate(f32[1,6,8,64,64]{4,3,2,1,0:T(8,128)} %convolution_bitcast_fusion.11, f32[1,6,8,64,64]{4,3,2,1,0:T(8,128)} %convolution_bitcast_fusion.10, f32[1,6,8,64,64]{4,3,2,1,0:T(8,128)} %convolution_bitcast_fusion.9, f32[1,6,8,64,64]{4,3,2,1,0:T(8,128)} %convolution_bitcast_fusion.8, ...), dimensions={4} | concatenate | bytes 7864320 | tf_op jit(solution)/shard_map/concatenate | solution.py:81
  56.7 3.4 %fusion.2 = f32[6,8,64]{2,1,0:T(8,128)S(1)} fusion(f32[1,6,8,64,320]{4,3,2,1,0:T(8,128)} %concatenate.116, f32[8,64,320]{2,1,0:T(8,128)S(1)} %bitcast.227, pred[6,320]{1,0:T(8,128)(4,1)S(1)} %add_compare_fusion), kind=kLoop, calls=%fused_computation.7 | loop fusion | flops 3929088 | bytes 4601728 | tf_op jit(solution)/shard_map/reduce_max | solution.py:83
  62.1 7.0 %concatenate.123 = f32[1,6,8,64,320]{4,3,2,1,0:T(8,128)} concatenate(f32[1,6,8,64,64]{4,3,2,1,0:T(8,128)} %convolution_bitcast_fusion.6, f32[1,6,8,64,64]{4,3,2,1,0:T(8,128)} %convolution_bitcast_fusion.5, f32[1,6,8,64,64]{4,3,2,1,0:T(8,128)} %convolution_bitcast_fusion.4, f32[1,6,8,64,64]{4,3,2,1,0:T(8,128)} %convolution_bitcast_fusion.3, ...), dimensions={4} | concatenate | bytes 7864320 | tf_op jit(solution)/shard_map/concatenate | solution.py:88
  69.1 4.9 %multiply_reduce_fusion = f32[6,8,64]{2,1,0:T(8,128)S(1)} fusion(f32[1,6,8,64,320]{4,3,2,1,0:T(8,128)} %concatenate.123, f32[6,8,64]{2,1,0:T(8,128)S(1)} %fusion.1, f32[6,8,64]{2,1,0:T(8,128)S(1)} %fusion.2, f32[8,64,320]{2,1,0:T(8,128)S(1)} %bitcast.229, f32[1,6,8,64,320]{4,3,2,1,0:T(8,128)} %concatenate.116, pred[6,320]{1,0:T(8,128)(4,1)S(1)} %add_compare_fusion), kind=kLoop, calls=%fused_computation.2 | loop fusion | flops 6878208 | bytes 8558464 | tf_op jit(solution)/shard_map/reduce_sum | solution.py:89
  74.2 5.5 %fusion.3 = (f32[8,64,320]{2,1,0:T(8,128)}, bf16[1,6,8,64,320]{4,3,2,1,0:T(8,128)(2,1)S(1)}, bf16[1,6,8,64,320]{4,3,2,1,0:T(8,128)(2,1)S(1)}) fusion(f32[1,6,8,64,320]{4,3,2,1,0:T(8,128)S(1)} %copy-done.3, f32[6,8,64]{2,1,0:T(8,128)S(1)} %multiply_reduce_fusion, f32[6,8,64]{2,1,0:T(8,128)S(1)} %fusion.1, f32[6,8,64]{2,1,0:T(8,128)S(1)} %fusion.2, ...), kind=kLoop, calls=%fused_computation.8 | loop fusion | flops 10649600 | bytes 13145984 | tf_op jit(solution)/shard_map/reduce_sum | solution.py:91
  97.3 1.8 slice.550
  101.3 2.3 %slice.537 = bf16[1,384,1024]{2,0,1:T(2,128)(2,1)} slice(f32[1,640,1024]{2,0,1:T(1,128)S(1)} %bitcast.232), slice={[0:1], [256:640], [0:1024]} | slice | bytes 1572864 | tf_op jit(solution)/shard_map/slice | solution.py:147
  103.6 2.2 %slice.548 = bf16[1,384,1024]{2,0,1:T(2,128)(2,1)} slice(f32[1,640,1024]{2,0,1:T(1,128)S(1)} %bitcast.235), slice={[0:1], [256:640], [0:1024]} | slice | bytes 1572864 | tf_op jit(solution)/shard_map/slice | solution.py:148
  107.2 2.1 %reshape.1137 = bf16[1,384,1024]{2,1,0:T(8,128)(2,1)} reshape(bf16[1,6,64,8,128]{4,3,2,1,0:T(8,128)(2,1)} %copy.104) | data formatting | bytes 1572864 | tf_op jit(solution)/shard_map/reshape | solution.py:149
  110.7 2.7 %reshape.1155 = f32[8,28608]{1,0:T(8,128)} reshape(f32[8,64,447]{2,1,0:T(8,128)} %maximum_maximum_fusion) | data formatting | bytes 1830912 | tf_op jit(solution)/shard_map/reshape | solution.py:53
  113.4 2.2 %concatenate.125 = f32[8,28672]{1,0:T(8,128)} pad(f32[8,28608]{1,0:T(8,128)} %reshape.1155, f32[]{:T(128)} %constant.322.clone.1), padding=0_0x0_64 | pad | bytes 1832964 | tf_op jit(solution)/shard_map/concatenate | solution.py:52
  115.6 2.7 %reshape.1156 = f32[8,64,448]{2,1,0:T(8,128)} reshape(f32[8,28672]{1,0:T(8,128)} %concatenate.125) | data formatting | bytes 1835008 | tf_op jit(solution)/shard_map/reshape | solution.py:55
  119.7 54.4 %psum.7 = f32[16,192]{1,0:T(8,128)} all-reduce(f32[16,192]{1,0:T(8,128)S(1)} %convolution_dynamic-update-slice_fusion), channel_id=1, replica_groups=mesh['sp'=16,'tp'=2] {'sp','tp'}, use_global_device_ids=true, to_apply=%region_5.6 | all-reduce | flops 3072 | bytes 24576 | tf_op jit(solution)/shard_map/psum | solution.py:162
  174.1 3.8 %fusion.14 = bf16[1,384,1024]{2,0,1:T(2,128)(2,1)} fusion(bf16[1,384,1024]{2,0,1:T(2,128)(2,1)} %slice.537, f32[1,256,1024]{2,0,1:T(1,128)} %collective-permute-done.2, f32[1,640,1024]{2,0,1:T(1,128)S(1)} %bitcast.233), kind=kLoop, calls=%fused_computation.46 | loop fusion | flops 262144 | bytes 3145728 | tf_op jit(solution)/shard_map/scatter-add | solution.py:147
  177.9 2.6 %copy.127 = bf16[1,384,1024]{2,1,0:T(8,128)(2,1)} copy(bf16[1,384,1024]{2,0,1:T(2,128)(2,1)} %fusion.14) | data formatting | bytes 1572864
  180.5 2.7 %fusion.13 = bf16[1,384,1024]{2,0,1:T(2,128)(2,1)S(1)} fusion(bf16[1,384,1024]{2,0,1:T(2,128)(2,1)S(1)} %copy-done.13, f32[1,256,1024]{2,0,1:T(1,128)} %collective-permute-done.3, f32[1,640,1024]{2,0,1:T(1,128)} %bitcast.236), kind=kLoop, calls=%fused_computation.44 | loop fusion | flops 262144 | bytes 3145728 | tf_op jit(solution)/shard_map/scatter-add | solution.py:148
  (95 shorter events, 49.9 us)
Async XLA Ops:
  0.6 13.0 %copy-start = (f32[8,192]{1,0:T(8,128)S(1)}, f32[8,192]{1,0:T(8,128)}, u32[]{:S(2)}) copy-start(f32[8,192]{1,0:T(8,128)} %param.32) | copy-start | bytes 18436
  0.6 13.2 %copy-start.16 = (bf16[1,384,1024]{2,1,0:T(8,128)(2,1)S(1)}, bf16[1,384,1024]{2,1,0:T(8,128)(2,1)}, u32[]{:S(2)}) copy-start(bf16[1,384,1024]{2,1,0:T(8,128)(2,1)} %param.33) | copy-start | bytes 2359300
  0.7 13.4 %copy-start.17 = (bf16[1,384,1024]{2,1,0:T(8,128)(2,1)S(1)}, bf16[1,384,1024]{2,1,0:T(8,128)(2,1)}, u32[]{:S(2)}) copy-start(bf16[1,384,1024]{2,1,0:T(8,128)(2,1)} %param.29) | copy-start | bytes 2359300
  2.7 17.5 %collective-permute-start = (bf16[1,256,1024]{2,1,0:T(8,128)(2,1)}, bf16[1,256,1024]{2,1,0:T(8,128)(2,1)}, u32[]{:S(2)}, u32[]{:S(2)}) collective-permute-start(bf16[1,256,1024]{2,1,0:T(8,128)(2,1)} %slice.478), channel_id=1, source_target_pairs={{0,2},{2,4},{4,6},{6,8},{8,10},{10,12},{12,14},{14,16},{16,18},{18... | collective-permute-start | bytes 1572872 | tf_op jit(solution)/shard_map/ppermute | solution.py:17
  10.2 20.0 %collective-permute-start.1 = (bf16[1,256,1024]{2,1,0:T(8,128)(2,1)}, bf16[1,256,1024]{2,1,0:T(8,128)(2,1)}, u32[]{:S(2)}, u32[]{:S(2)}) collective-permute-start(bf16[1,256,1024]{2,1,0:T(8,128)(2,1)} %slice.486), channel_id=1, source_target_pairs={{0,2},{2,4},{4,6},{6,8},{8,10},{10,12},{12,14},{14,16},{16,18},{18... | collective-permute-start | bytes 1572872 | tf_op jit(solution)/shard_map/ppermute | solution.py:17
  21.9 8.4 %copy-start.15 = (bf16[1,384,1024]{2,1,0:T(8,128)(2,1)S(1)}, bf16[1,384,1024]{2,1,0:T(8,128)(2,1)}, u32[]{:S(2)}) copy-start(bf16[1,384,1024]{2,1,0:T(8,128)(2,1)} %param.31) | copy-start | bytes 2359300
  22.8 20.1 %copy-start.7 = (bf16[1,6,64,8,128]{4,3,2,1,0:T(8,128)(2,1)}, bf16[1,6,64,8,128]{4,3,2,1,0:T(8,128)(2,1)S(1)}, u32[]{:S(2)}) copy-start(bf16[1,6,64,8,128]{4,3,2,1,0:T(8,128)(2,1)S(1)} %get-tuple-element.162) | copy-start | bytes 2359300
  22.8 21.8 %copy-start.9 = (bf16[1,6,64,8,128]{4,3,2,1,0:T(8,128)(2,1)}, bf16[1,6,64,8,128]{4,3,2,1,0:T(8,128)(2,1)S(1)}, u32[]{:S(2)}) copy-start(bf16[1,6,64,8,128]{4,3,2,1,0:T(8,128)(2,1)S(1)} %get-tuple-element.161) | copy-start | bytes 2359300
  22.8 23.5 %copy-start.11 = (bf16[1,6,64,8,128]{4,3,2,1,0:T(8,128)(2,1)}, bf16[1,6,64,8,128]{4,3,2,1,0:T(8,128)(2,1)S(1)}, u32[]{:S(2)}) copy-start(bf16[1,6,64,8,128]{4,3,2,1,0:T(8,128)(2,1)S(1)} %get-tuple-element.160) | copy-start | bytes 2359300
  22.8 25.3 %copy-start.5 = (bf16[1,6,64,8,128]{4,3,2,1,0:T(8,128)(2,1)}, bf16[1,6,64,8,128]{4,3,2,1,0:T(8,128)(2,1)S(1)}, u32[]{:S(2)}) copy-start(bf16[1,6,64,8,128]{4,3,2,1,0:T(8,128)(2,1)S(1)} %get-tuple-element.159) | copy-start | bytes 2359300
  56.7 3.8 %copy-start.2 = (f32[1,6,8,64,320]{4,3,2,1,0:T(8,128)S(1)}, f32[1,6,8,64,320]{4,3,2,1,0:T(8,128)}, u32[]{:S(2)}) copy-start(f32[1,6,8,64,320]{4,3,2,1,0:T(8,128)} %concatenate.116) | copy-start | bytes 11796484
  69.1 5.1 %copy-start.3 = (f32[1,6,8,64,320]{4,3,2,1,0:T(8,128)S(1)}, f32[1,6,8,64,320]{4,3,2,1,0:T(8,128)}, u32[]{:S(2)}) copy-start(f32[1,6,8,64,320]{4,3,2,1,0:T(8,128)} %concatenate.123) | copy-start | bytes 11796484
  74.2 5.5 %copy-start.12 = (bf16[1,6,64,8,128]{4,3,2,1,0:T(8,128)(2,1)S(1)}, bf16[1,6,64,8,128]{4,3,2,1,0:T(8,128)(2,1)}, u32[]{:S(2)}) copy-start(bf16[1,6,64,8,128]{4,3,2,1,0:T(8,128)(2,1)} %copy-done.11) | copy-start | bytes 2359300
  79.7 1.1 copy-start.10
  89.1 85.1 %collective-permute-start.2 = (f32[1,256,1024]{2,0,1:T(1,128)}, f32[1,256,1024]{2,0,1:T(1,128)}, u32[]{:S(2)}, u32[]{:S(2)}) collective-permute-start(f32[1,256,1024]{2,0,1:T(1,128)} %slice.539), channel_id=1, source_target_pairs={{2,0},{4,2},{6,4},{8,6},{10,8},{12,10},{14,12},{16,14},{18,16},{20... | collective-permute-start | bytes 3145736 | tf_op jit(solution)/shard_map/ppermute | solution.py:17
  94.1 1.1 copy-start.8
  97.3 6.3 %copy-start.4 = (f32[1,10,64,8,128]{4,3,0,2,1:T(8,128)}, f32[1,10,64,8,128]{4,3,0,2,1:T(8,128)S(1)}, u32[]{:S(2)}) copy-start(f32[1,10,64,8,128]{4,3,0,2,1:T(8,128)S(1)} %copy.126) | copy-start | bytes 7864324
  97.3 3.4 %copy-start.6 = (bf16[1,6,64,8,128]{4,3,2,1,0:T(8,128)(2,1)S(1)}, bf16[1,6,64,8,128]{4,3,2,1,0:T(8,128)(2,1)}, u32[]{:S(2)}) copy-start(bf16[1,6,64,8,128]{4,3,2,1,0:T(8,128)(2,1)} %copy-done.5) | copy-start | bytes 2359300
  99.1 81.4 %collective-permute-start.3 = (f32[1,256,1024]{2,0,1:T(1,128)}, f32[1,256,1024]{2,0,1:T(1,128)}, u32[]{:S(2)}, u32[]{:S(2)}) collective-permute-start(f32[1,256,1024]{2,0,1:T(1,128)} %slice.550), channel_id=1, source_target_pairs={{2,0},{4,2},{6,4},{8,6},{10,8},{12,10},{14,12},{16,14},{18,16},{20... | collective-permute-start | bytes 3145736 | tf_op jit(solution)/shard_map/ppermute | solution.py:17
  105.8 3.5 %copy-start.14 = (f32[8,64,320]{2,1,0:T(8,128)S(1)}, f32[8,64,320]{2,1,0:T(8,128)}, u32[]{:S(2)}) copy-start(f32[8,64,320]{2,1,0:T(8,128)} %get-tuple-element.156) | copy-start | bytes 1966084
  174.1 6.4 %copy-start.13 = (bf16[1,384,1024]{2,0,1:T(2,128)(2,1)S(1)}, bf16[1,384,1024]{2,0,1:T(2,128)(2,1)}, u32[]{:S(2)}) copy-start(bf16[1,384,1024]{2,0,1:T(2,128)(2,1)} %slice.548) | copy-start | bytes 2359300
  177.9 6.4 %copy-start.1 = (f32[8,192]{1,0:T(8,128)S(1)}, f32[8,192]{1,0:T(8,128)}, u32[]{:S(2)}) copy-start(f32[8,192]{1,0:T(8,128)} %param.32) | copy-start | bytes 18436
where the time goes:
time: 185 us; the launch traced here: 184 us
  blocking collectives  54.4 us (29%)
  local copies, waits for them, and re-layouts  52.7 us (28%)
  matrix products  27.5 us (15%)
  other arithmetic  27.1 us (15%)
  starting transfers between devices  12.1 us (7%)
  waiting for transfers between devices  9.53 us (5%)
    psum x1, blocking collectives, local(): bias_grad = lax.psum(full_table, ('sp', 'tp'))  54.4 us
    ppermute x4, starting transfers between devices, from_behind(): lax.ppermute(value, axis, [(source, source + steps) for source in range(l...  12.1 us
    ppermute x4, waiting for transfers between devices, from_behind(): lax.ppermute(value, axis, [(source, source + steps) for source in range(l...  9.53 us
    dot_general x5, matrix products, band_core(): jnp.einsum('sncha,snkha->snhck', q_segs, k_band[:, offset:offset + seg_co...  8.59 us
    dot_general x5, matrix products, band_core(): jnp.einsum('sncha,snkha->snhck', g_segs, v_band[:, offset:offset + seg_co...  8.5 us
    concatenate x1, local copies, waits for them, and re-layouts, band_core(): prob_grad = jnp.concatenate(prob_parts, axis=-1)  7.01 us
    concatenate x1, local copies, waits for them, and re-layouts, band_core(): jnp.concatenate(score_parts, axis=-1) * score_scale + table[None, None]  6.93 us
    unnamed x42, local copies, waits for them, and re-layouts  6.5 us
  transfers between devices with their start and end apart: 4, of which 2 were waited for; matrix products, arithmetic and copies ran while one was open for 23% of the time, Pallas kernels for 0%

commit v1 on v0

--- a/solution.py
+++ b/solution.py
@@ -159,7 +159,7 @@
     full_table = lax.dynamic_update_slice_in_dim(
         full_table, local_bias, lax.axis_index("tp") * head_count, 0
     )
-    bias_grad = lax.psum(full_table, ("sp", "tp"))
+    bias_grad = jax.lax.psum(jax.lax.psum(full_table, "tp"), "sp")
     return (query_grad, key_grad, value_grad, bias_grad)
 
 

time: 185 us -> 220 us (1.19)
  blocking collectives: 54.4 us -> 88.9 us
    psum x1 -> x2, blocking collectives: 54.4 us -> 88.9 us  [local(): bias_grad = jax.lax.psum(jax.lax.psum(full_table, 'tp'), 'sp')]
  transfers between devices with their start and end apart: 4 -> 4, of which waited for: 2 -> 2; matrix products, arithmetic and copies ran while one was open for 23% -> 19% of each run, Pallas kernels for 0% -> 0%
where the time goes in v1:
time: 220 us; the launch traced here: 219 us
  blocking collectives  88.9 us (40%)
  local copies, waits for them, and re-layouts  53 us (24%)
  matrix products  27.5 us (12%)
  other arithmetic  27.1 us (12%)
  starting transfers between devices  11.8 us (5%)
  waiting for transfers between devices  9.51 us (4%)
    psum x2, blocking collectives, local(): bias_grad = jax.lax.psum(jax.lax.psum(full_table, 'tp'), 'sp')  88.9 us
    ppermute x4, starting transfers between devices, from_behind(): lax.ppermute(value, axis, [(source, source + steps) for source in range(l...  11.8 us
    ppermute x4, waiting for transfers between devices, from_behind(): lax.ppermute(value, axis, [(source, source + steps) for source in range(l...  9.51 us
    dot_general x5, matrix products, band_core(): jnp.einsum('sncha,snkha->snhck', q_segs, k_band[:, offset:offset + seg_co...  8.55 us
    dot_general x5, matrix products, band_core(): jnp.einsum('sncha,snkha->snhck', g_segs, v_band[:, offset:offset + seg_co...  8.5 us
    concatenate x1, local copies, waits for them, and re-layouts, band_core(): prob_grad = jnp.concatenate(prob_parts, axis=-1)  7.01 us
    concatenate x1, local copies, waits for them, and re-layouts, band_core(): jnp.concatenate(score_parts, axis=-1) * score_scale + table[None, None]  6.94 us
    unnamed x42, local copies, waits for them, and re-layouts  6.86 us
  transfers between devices with their start and end apart: 4, of which 2 were waited for; matrix products, arithmetic and copies ran while one was open for 19% of the time, Pallas kernels for 0%

profile of v1, /device:TPU:0, one launch (start us, length us, event | category | flops | bytes accessed | tf_op | source)
XLA Modules:
  0.0 218.8 jit_solution(13255046188366286213)
XLA Ops:
  0.7 2.0 slice.478
  2.7 5.7 %collective-permute-start = (bf16[1,256,1024]{2,1,0:T(8,128)(2,1)}, bf16[1,256,1024]{2,1,0:T(8,128)(2,1)}, u32[]{:S(2)}, u32[]{:S(2)}) collective-permute-start(bf16[1,256,1024]{2,1,0:T(8,128)(2,1)} %slice.478), channel_id=1, source_target_pairs={{0,2},{2,4},{4,6},{6,8},{8,10},{10,12},{12,14},{14,16},{16,18},{18... | collective-permute-start | bytes 1572872 | tf_op jit(solution)/shard_map/ppermute | solution.py:17
  8.3 1.9 slice.486
  10.2 3.4 %collective-permute-start.1 = (bf16[1,256,1024]{2,1,0:T(8,128)(2,1)}, bf16[1,256,1024]{2,1,0:T(8,128)(2,1)}, u32[]{:S(2)}, u32[]{:S(2)}) collective-permute-start(bf16[1,256,1024]{2,1,0:T(8,128)(2,1)} %slice.486), channel_id=1, source_target_pairs={{0,2},{2,4},{4,6},{6,8},{8,10},{10,12},{12,14},{14,16},{16,18},{18... | collective-permute-start | bytes 1572872 | tf_op jit(solution)/shard_map/ppermute | solution.py:17
  16.0 2.0 reshape.1124
  18.1 2.1 collective-permute-done
  22.8 7.4 %collective-permute-done.1 = bf16[1,256,1024]{2,1,0:T(8,128)(2,1)} collective-permute-done((bf16[1,256,1024]{2,1,0:T(8,128)(2,1)}, bf16[1,256,1024]{2,1,0:T(8,128)(2,1)}, u32[]{:S(2)}, u32[]{:S(2)}) %collective-permute-start.1) | collective-permute-done | bytes 524320 | tf_op jit(solution)/shard_map/ppermute | solution.py:17
  44.5 1.8 convolution_bitcast_fusion.9
  49.7 6.9 %concatenate.116 = f32[1,6,8,64,320]{4,3,2,1,0:T(8,128)} concatenate(f32[1,6,8,64,64]{4,3,2,1,0:T(8,128)} %convolution_bitcast_fusion.11, f32[1,6,8,64,64]{4,3,2,1,0:T(8,128)} %convolution_bitcast_fusion.10, f32[1,6,8,64,64]{4,3,2,1,0:T(8,128)} %convolution_bitcast_fusion.9, f32[1,6,8,64,64]{4,3,2,1,0:T(8,128)} %convolution_bitcast_fusion.8, ...), dimensions={4} | concatenate | bytes 7864320 | tf_op jit(solution)/shard_map/concatenate | solution.py:81
  56.6 3.4 %fusion.2 = f32[6,8,64]{2,1,0:T(8,128)S(1)} fusion(f32[1,6,8,64,320]{4,3,2,1,0:T(8,128)} %concatenate.116, f32[8,64,320]{2,1,0:T(8,128)S(1)} %bitcast.227, pred[6,320]{1,0:T(8,128)(4,1)S(1)} %add_compare_fusion), kind=kLoop, calls=%fused_computation.7 | loop fusion | flops 3929088 | bytes 4601728 | tf_op jit(solution)/shard_map/reduce_max | solution.py:83
  62.0 7.0 %concatenate.123 = f32[1,6,8,64,320]{4,3,2,1,0:T(8,128)} concatenate(f32[1,6,8,64,64]{4,3,2,1,0:T(8,128)} %convolution_bitcast_fusion.6, f32[1,6,8,64,64]{4,3,2,1,0:T(8,128)} %convolution_bitcast_fusion.5, f32[1,6,8,64,64]{4,3,2,1,0:T(8,128)} %convolution_bitcast_fusion.4, f32[1,6,8,64,64]{4,3,2,1,0:T(8,128)} %convolution_bitcast_fusion.3, ...), dimensions={4} | concatenate | bytes 7864320 | tf_op jit(solution)/shard_map/concatenate | solution.py:88
  69.0 4.9 %multiply_reduce_fusion = f32[6,8,64]{2,1,0:T(8,128)S(1)} fusion(f32[1,6,8,64,320]{4,3,2,1,0:T(8,128)} %concatenate.123, f32[6,8,64]{2,1,0:T(8,128)S(1)} %fusion.1, f32[6,8,64]{2,1,0:T(8,128)S(1)} %fusion.2, f32[8,64,320]{2,1,0:T(8,128)S(1)} %bitcast.229, f32[1,6,8,64,320]{4,3,2,1,0:T(8,128)} %concatenate.116, pred[6,320]{1,0:T(8,128)(4,1)S(1)} %add_compare_fusion), kind=kLoop, calls=%fused_computation.2 | loop fusion | flops 6878208 | bytes 8558464 | tf_op jit(solution)/shard_map/reduce_sum | solution.py:89
  74.1 5.5 %fusion.3 = (f32[8,64,320]{2,1,0:T(8,128)}, bf16[1,6,8,64,320]{4,3,2,1,0:T(8,128)(2,1)S(1)}, bf16[1,6,8,64,320]{4,3,2,1,0:T(8,128)(2,1)S(1)}) fusion(f32[1,6,8,64,320]{4,3,2,1,0:T(8,128)S(1)} %copy-done.3, f32[6,8,64]{2,1,0:T(8,128)S(1)} %multiply_reduce_fusion, f32[6,8,64]{2,1,0:T(8,128)S(1)} %fusion.1, f32[6,8,64]{2,1,0:T(8,128)S(1)} %fusion.2, ...), kind=kLoop, calls=%fused_computation.8 | loop fusion | flops 10649600 | bytes 13145984 | tf_op jit(solution)/shard_map/reduce_sum | solution.py:91
  101.3 2.3 %slice.537 = bf16[1,384,1024]{2,0,1:T(2,128)(2,1)} slice(f32[1,640,1024]{2,0,1:T(1,128)S(1)} %bitcast.232), slice={[0:1], [256:640], [0:1024]} | slice | bytes 1572864 | tf_op jit(solution)/shard_map/slice | solution.py:147
  103.6 2.2 %slice.548 = bf16[1,384,1024]{2,0,1:T(2,128)(2,1)} slice(f32[1,640,1024]{2,0,1:T(1,128)S(1)} %bitcast.235), slice={[0:1], [256:640], [0:1024]} | slice | bytes 1572864 | tf_op jit(solution)/shard_map/slice | solution.py:148
  107.2 2.1 reshape.1137
  110.7 2.7 %reshape.1155 = f32[8,28608]{1,0:T(8,128)} reshape(f32[8,64,447]{2,1,0:T(8,128)} %maximum_maximum_fusion) | data formatting | bytes 1830912 | tf_op jit(solution)/shard_map/reshape | solution.py:53
  113.4 2.2 concatenate.125
  115.6 2.7 %reshape.1156 = f32[8,64,448]{2,1,0:T(8,128)} reshape(f32[8,28672]{1,0:T(8,128)} %concatenate.125) | data formatting | bytes 1835008 | tf_op jit(solution)/shard_map/reshape | solution.py:55
  119.7 3.4 %psum.14 = f32[16,192]{1,0:T(8,128)S(1)} all-reduce(f32[16,192]{1,0:T(8,128)S(1)} %convolution_dynamic-update-slice_fusion), channel_id=1, replica_groups=mesh['sp'=16,'tp'=2] {'tp'}, use_global_device_ids=true, to_apply=%region_5.6 | all-reduce | flops 3072 | bytes 24576 | tf_op jit(solution)/shard_map/psum | solution.py:162
  123.1 85.5 %psum.15 = f32[16,192]{1,0:T(8,128)} all-reduce(f32[16,192]{1,0:T(8,128)S(1)} %psum.14), channel_id=1, replica_groups=mesh['sp'=16,'tp'=2] {'sp'}, use_global_device_ids=true, to_apply=%region_6.7 | all-reduce | flops 3072 | bytes 24576 | tf_op jit(solution)/shard_map/psum | solution.py:162
  208.6 3.8 %fusion.14 = bf16[1,384,1024]{2,0,1:T(2,128)(2,1)} fusion(bf16[1,384,1024]{2,0,1:T(2,128)(2,1)} %slice.537, f32[1,256,1024]{2,0,1:T(1,128)} %collective-permute-done.2, f32[1,640,1024]{2,0,1:T(1,128)S(1)} %bitcast.233), kind=kLoop, calls=%fused_computation.46 | loop fusion | flops 262144 | bytes 3145728 | tf_op jit(solution)/shard_map/scatter-add | solution.py:147
  212.4 2.6 %copy.127 = bf16[1,384,1024]{2,1,0:T(8,128)(2,1)} copy(bf16[1,384,1024]{2,0,1:T(2,128)(2,1)} %fusion.14) | data formatting | bytes 1572864
  215.0 2.7 %fusion.13 = bf16[1,384,1024]{2,0,1:T(2,128)(2,1)S(1)} fusion(bf16[1,384,1024]{2,0,1:T(2,128)(2,1)S(1)} %copy-done.13, f32[1,256,1024]{2,0,1:T(1,128)} %collective-permute-done.3, f32[1,640,1024]{2,0,1:T(1,128)} %bitcast.236), kind=kLoop, calls=%fused_computation.44 | loop fusion | flops 262144 | bytes 3145728 | tf_op jit(solution)/shard_map/scatter-add | solution.py:148
  (96 shorter events, 51.7 us)
Async XLA Ops:
  0.6 13.0 %copy-start = (f32[8,192]{1,0:T(8,128)S(1)}, f32[8,192]{1,0:T(8,128)}, u32[]{:S(2)}) copy-start(f32[8,192]{1,0:T(8,128)} %param.32) | copy-start | bytes 18436
  0.6 13.3 %copy-start.16 = (bf16[1,384,1024]{2,1,0:T(8,128)(2,1)S(1)}, bf16[1,384,1024]{2,1,0:T(8,128)(2,1)}, u32[]{:S(2)}) copy-start(bf16[1,384,1024]{2,1,0:T(8,128)(2,1)} %param.33) | copy-start | bytes 2359300
  0.7 13.4 %copy-start.17 = (bf16[1,384,1024]{2,1,0:T(8,128)(2,1)S(1)}, bf16[1,384,1024]{2,1,0:T(8,128)(2,1)}, u32[]{:S(2)}) copy-start(bf16[1,384,1024]{2,1,0:T(8,128)(2,1)} %param.29) | copy-start | bytes 2359300
  2.7 17.5 %collective-permute-start = (bf16[1,256,1024]{2,1,0:T(8,128)(2,1)}, bf16[1,256,1024]{2,1,0:T(8,128)(2,1)}, u32[]{:S(2)}, u32[]{:S(2)}) collective-permute-start(bf16[1,256,1024]{2,1,0:T(8,128)(2,1)} %slice.478), channel_id=1, source_target_pairs={{0,2},{2,4},{4,6},{6,8},{8,10},{10,12},{12,14},{14,16},{16,18},{18... | collective-permute-start | bytes 1572872 | tf_op jit(solution)/shard_map/ppermute | solution.py:17
  10.2 20.0 %collective-permute-start.1 = (bf16[1,256,1024]{2,1,0:T(8,128)(2,1)}, bf16[1,256,1024]{2,1,0:T(8,128)(2,1)}, u32[]{:S(2)}, u32[]{:S(2)}) collective-permute-start(bf16[1,256,1024]{2,1,0:T(8,128)(2,1)} %slice.486), channel_id=1, source_target_pairs={{0,2},{2,4},{4,6},{6,8},{8,10},{10,12},{12,14},{14,16},{16,18},{18... | collective-permute-start | bytes 1572872 | tf_op jit(solution)/shard_map/ppermute | solution.py:17
  21.9 8.4 %copy-start.15 = (bf16[1,384,1024]{2,1,0:T(8,128)(2,1)S(1)}, bf16[1,384,1024]{2,1,0:T(8,128)(2,1)}, u32[]{:S(2)}) copy-start(bf16[1,384,1024]{2,1,0:T(8,128)(2,1)} %param.31) | copy-start | bytes 2359300
  22.8 18.4 %copy-start.7 = (bf16[1,6,64,8,128]{4,3,2,1,0:T(8,128)(2,1)}, bf16[1,6,64,8,128]{4,3,2,1,0:T(8,128)(2,1)S(1)}, u32[]{:S(2)}) copy-start(bf16[1,6,64,8,128]{4,3,2,1,0:T(8,128)(2,1)S(1)} %get-tuple-element.163) | copy-start | bytes 2359300
  22.8 21.8 %copy-start.9 = (bf16[1,6,64,8,128]{4,3,2,1,0:T(8,128)(2,1)}, bf16[1,6,64,8,128]{4,3,2,1,0:T(8,128)(2,1)S(1)}, u32[]{:S(2)}) copy-start(bf16[1,6,64,8,128]{4,3,2,1,0:T(8,128)(2,1)S(1)} %get-tuple-element.161) | copy-start | bytes 2359300
  22.8 23.5 %copy-start.11 = (bf16[1,6,64,8,128]{4,3,2,1,0:T(8,128)(2,1)}, bf16[1,6,64,8,128]{4,3,2,1,0:T(8,128)(2,1)S(1)}, u32[]{:S(2)}) copy-start(bf16[1,6,64,8,128]{4,3,2,1,0:T(8,128)(2,1)S(1)} %get-tuple-element.160) | copy-start | bytes 2359300
  22.8 25.2 %copy-start.5 = (bf16[1,6,64,8,128]{4,3,2,1,0:T(8,128)(2,1)}, bf16[1,6,64,8,128]{4,3,2,1,0:T(8,128)(2,1)S(1)}, u32[]{:S(2)}) copy-start(bf16[1,6,64,8,128]{4,3,2,1,0:T(8,128)(2,1)S(1)} %get-tuple-element.159) | copy-start | bytes 2359300
  56.6 3.8 %copy-start.2 = (f32[1,6,8,64,320]{4,3,2,1,0:T(8,128)S(1)}, f32[1,6,8,64,320]{4,3,2,1,0:T(8,128)}, u32[]{:S(2)}) copy-start(f32[1,6,8,64,320]{4,3,2,1,0:T(8,128)} %concatenate.116) | copy-start | bytes 11796484
  69.0 5.1 %copy-start.3 = (f32[1,6,8,64,320]{4,3,2,1,0:T(8,128)S(1)}, f32[1,6,8,64,320]{4,3,2,1,0:T(8,128)}, u32[]{:S(2)}) copy-start(f32[1,6,8,64,320]{4,3,2,1,0:T(8,128)} %concatenate.123) | copy-start | bytes 11796484
  74.1 5.5 %copy-start.12 = (bf16[1,6,64,8,128]{4,3,2,1,0:T(8,128)(2,1)S(1)}, bf16[1,6,64,8,128]{4,3,2,1,0:T(8,128)(2,1)}, u32[]{:S(2)}) copy-start(bf16[1,6,64,8,128]{4,3,2,1,0:T(8,128)(2,1)} %copy-done.11) | copy-start | bytes 2359300
  79.6 1.1 copy-start.10
  80.8 1.1 copy-start.8
  90.3 118.3 %collective-permute-start.2 = (f32[1,256,1024]{2,0,1:T(1,128)}, f32[1,256,1024]{2,0,1:T(1,128)}, u32[]{:S(2)}, u32[]{:S(2)}) collective-permute-start(f32[1,256,1024]{2,0,1:T(1,128)} %slice.539), channel_id=1, source_target_pairs={{2,0},{4,2},{6,4},{8,6},{10,8},{12,10},{14,12},{16,14},{18,16},{20... | collective-permute-start | bytes 3145736 | tf_op jit(solution)/shard_map/ppermute | solution.py:17
  97.6 5.9 %copy-start.4 = (f32[1,10,64,8,128]{4,3,0,2,1:T(8,128)}, f32[1,10,64,8,128]{4,3,0,2,1:T(8,128)S(1)}, u32[]{:S(2)}) copy-start(f32[1,10,64,8,128]{4,3,0,2,1:T(8,128)S(1)} %copy.126) | copy-start | bytes 7864324
  97.6 3.0 %copy-start.6 = (bf16[1,6,64,8,128]{4,3,2,1,0:T(8,128)(2,1)S(1)}, bf16[1,6,64,8,128]{4,3,2,1,0:T(8,128)(2,1)}, u32[]{:S(2)}) copy-start(bf16[1,6,64,8,128]{4,3,2,1,0:T(8,128)(2,1)} %copy-done.5) | copy-start | bytes 2359300
  99.3 115.6 %collective-permute-start.3 = (f32[1,256,1024]{2,0,1:T(1,128)}, f32[1,256,1024]{2,0,1:T(1,128)}, u32[]{:S(2)}, u32[]{:S(2)}) collective-permute-start(f32[1,256,1024]{2,0,1:T(1,128)} %slice.550), channel_id=1, source_target_pairs={{2,0},{4,2},{6,4},{8,6},{10,8},{12,10},{14,12},{16,14},{18,16},{20... | collective-permute-start | bytes 3145736 | tf_op jit(solution)/shard_map/ppermute | solution.py:17
  105.8 3.5 %copy-start.14 = (f32[8,64,320]{2,1,0:T(8,128)S(1)}, f32[8,64,320]{2,1,0:T(8,128)}, u32[]{:S(2)}) copy-start(f32[8,64,320]{2,1,0:T(8,128)} %get-tuple-element.156) | copy-start | bytes 1966084
  208.6 6.4 %copy-start.13 = (bf16[1,384,1024]{2,0,1:T(2,128)(2,1)S(1)}, bf16[1,384,1024]{2,0,1:T(2,128)(2,1)}, u32[]{:S(2)}) copy-start(bf16[1,384,1024]{2,0,1:T(2,128)(2,1)} %slice.548) | copy-start | bytes 2359300
  212.4 6.4 %copy-start.1 = (f32[8,192]{1,0:T(8,128)S(1)}, f32[8,192]{1,0:T(8,128)}, u32[]{:S(2)}) copy-start(f32[8,192]{1,0:T(8,128)} %param.32) | copy-start | bytes 18436
